TPU v7x, 32 devices: a whole 2x2x4 slice. The times are simulated.
32 devices in a mesh: sp: 16 (over z, y, x), tp: 2 (over core).
Axes of the slice: x: 2, y: 2, z: 4, core: 2. Of those that a mesh axis runs over, the one named last changes fastest.
Arguments:
- resid: bfloat16 [2048, 2048], P(('sp', 'tp')), may hold values from -3 to 3
- queries: bfloat16 [2048, 2048], P('sp', 'tp'), may hold values from -6 to 6
- keys: bfloat16 [2048, 2048], P('sp', 'tp'), may hold values from -6 to 6
- values: bfloat16 [2048, 2048], P('sp', 'tp'), may hold values from -8 to 8
- doc_ids: int32 [2048], P('sp'), may hold values from 0 to 3, never falling along the last dimension, each value on 1 to 896 neighbouring positions
- score_offset: float32 [32], P('tp'), may hold values from -10 to -3
- out_weight: bfloat16 [2048, 2048], P('tp'), may hold values from -0.1875 to 0.1875
- norm_gain: float32 [2048], replicated, may hold values from 0.1 to 1.9
- gate_weight: bfloat16 [2048, 6144], P('sp', 'tp'), may hold values from -0.125 to 0.125
- up_weight: bfloat16 [2048, 6144], P('sp', 'tp'), may hold values from -0.125 to 0.125
- down_weight: bfloat16 [6144, 2048], P('tp', 'sp'), may hold values from -0.078125 to 0.078125
Outputs:
- layer_out: bfloat16 [2048, 2048], P(('sp', 'tp'))
Inputs may be any that keep to these rules, and one draw needn't show every extreme that they name: `doc_ids`: document numbers never fall along the sequence; each document has 1 to 896 positions, and one has exactly 896.
All inputs are finite; a program needn't handle non-finite values.
Results may differ from a plain program's by a relative error of at most 0.017.
Values may be sent and summed in bfloat16 or wider, within the bound.
A program may use at most 128 MiB of HBM per device.

v0:
```python
import jax
import jax.numpy as jnp
from jax import lax
from jax.sharding import PartitionSpec as P


def from_behind(shard, axis, by):
    peers = lax.axis_size(axis)
    pairs = [(i, i + by) for i in range(peers) if 0 <= i + by < peers]
    return lax.ppermute(shard, axis, pairs)


def as_sent(shard):
    return jax.tree.map(lambda a: a.astype(jnp.bfloat16) if a.dtype == jnp.float32 else a, shard)


def joined(earlier, later):
    return (
        jnp.concatenate([earlier[0], later[0]], axis=0),
        jnp.concatenate([earlier[1], later[1]], axis=0),
        jnp.concatenate([earlier[2], later[2]], axis=0),
    )


def block_update(carry, block, start, context):
    queries_h, q_pos, q_docs, offsets, scale = context
    total, carried = carry
    k_block, v_block, d_block = block
    count = k_block.shape[0]
    heads = offsets.shape[0]
    head_dim = queries_h.shape[2]

    def compute():
        key_pos = start + jnp.arange(count, dtype=jnp.int32)
        live = (
            (key_pos[None, :] >= 0)
            & (key_pos[None, :] < q_pos[:, None])
            & (d_block[None, :] == q_docs[:, None])
        )
        k_heads = k_block.reshape(count, heads, head_dim)
        v_heads = v_block.reshape(count, heads, head_dim)
        scores = (
            jnp.einsum("thd,shd->hts", queries_h, k_heads, preferred_element_type=jnp.float32)
            * scale
            + offsets[:, None, None]
        )
        log_keep = jnp.where(live[None], jax.nn.log_sigmoid(-scores), 0.0)
        tail = lax.cumsum(log_keep, axis=2, reverse=True) - log_keep + carried[:, :, None]
        weight = jnp.where(live[None], jnp.exp(jax.nn.log_sigmoid(scores) + tail), 0.0).astype(
            jnp.bfloat16
        )
        added = jnp.einsum("hts,shd->thd", weight, v_heads, preferred_element_type=jnp.float32)
        return (total + added, carried + jnp.sum(log_keep, axis=2))

    reached = (start + count > 0) & (d_block[-1] >= q_docs[0])
    return lax.cond(reached, compute, lambda: carry)


def on_device(
    resid,
    queries,
    keys,
    values,
    doc_ids,
    score_offset,
    out_weight,
    norm_gain,
    gate_weight,
    up_weight,
    down_weight,
):
    rows = queries.shape[0]
    heads = score_offset.shape[0]
    head_dim = queries.shape[1] // heads
    base = lax.axis_index("sp") * rows
    q_pos = base + jnp.arange(rows, dtype=jnp.int32)
    context = (
        queries.reshape(rows, heads, head_dim),
        q_pos,
        doc_ids,
        score_offset,
        head_dim ** (-0.5),
    )
    own = (keys, values, doc_ids)
    carry = (jnp.zeros((rows, heads, head_dim), jnp.float32), jnp.zeros((heads, rows), jnp.float32))
    nearest = from_behind((keys, values, doc_ids), "sp", 1)
    paired = joined(nearest, own)
    carry = block_update(carry, paired, base - rows, context)
    middle = from_behind((paired[0], paired[1], as_sent(paired[2])), "sp", 2)
    carry = block_update(carry, middle, base - 3 * rows, context)
    fourfold = joined(middle, paired)
    farthest = from_behind((fourfold[0], fourfold[1], as_sent(fourfold[2])), "sp", 4)
    carry = block_update(
        carry, tuple((piece[2 * rows :] for piece in farthest)), base - 5 * rows, context
    )
    carry = block_update(
        carry, tuple((piece[: 2 * rows] for piece in farthest)), base - 7 * rows, context
    )
    attended = carry[0].reshape(rows, heads * head_dim).astype(jnp.bfloat16)
    mixed_attn = lax.psum_scatter(
        jnp.dot(attended, out_weight, preferred_element_type=jnp.float32).astype(jnp.bfloat16),
        "tp",
        scatter_dimension=0,
        tiled=True,
    ).astype(jnp.float32)
    stream = resid.astype(jnp.float32) + mixed_attn
    normed = (
        stream * lax.rsqrt(jnp.mean(stream * stream, axis=1, keepdims=True) + 1e-06) * norm_gain
    ).astype(jnp.bfloat16)
    span_rows = lax.all_gather(normed, "tp", axis=0, tiled=True)
    gate = jnp.dot(
        span_rows,
        lax.all_gather(gate_weight, "sp", axis=0, tiled=True),
        preferred_element_type=jnp.float32,
    )
    upper = jnp.dot(
        span_rows,
        lax.all_gather(up_weight, "sp", axis=0, tiled=True),
        preferred_element_type=jnp.float32,
    )
    hidden = (jax.nn.silu(gate) * upper).astype(jnp.bfloat16)
    partial_out = jnp.dot(
        hidden,
        lax.all_gather(down_weight, "sp", axis=1, tiled=True),
        preferred_element_type=jnp.float32,
    )
    feed = lax.psum_scatter(
        partial_out.astype(jnp.bfloat16), "tp", scatter_dimension=0, tiled=True
    ).astype(jnp.float32)
    return (stream + feed).astype(jnp.bfloat16)


def solution(mesh):
    in_specs = (
        P(("sp", "tp"), None),
        P("sp", "tp"),
        P("sp", "tp"),
        P("sp", "tp"),
        P("sp"),
        P("tp"),
        P("tp", None),
        P(),
        P("sp", "tp"),
        P("sp", "tp"),
        P("tp", "sp"),
    )
    out_specs = P(("sp", "tp"), None)
    return jax.shard_map(
        on_device, mesh=mesh, in_specs=in_specs, out_specs=out_specs, check_vma=False
    )
```

profile of v0, /device:TPU:0, one launch (start us, length us, event | category | flops | bytes accessed | tf_op | source)
XLA Modules:
  0.0 761.2 jit_solution(9639619573280566356)
XLA Ops:
  7.4 1.1 copy.23
  8.5 4.9 collective-permute-start.4
  13.4 1.1 copy.20
  14.5 3.4 collective-permute-start.3
  17.9 2.1 collective-permute-done.4
  20.1 5.3 collective-permute-start.6
  25.6 4.6 collective-permute-start.5
  30.2 7.5 collective-permute-done.6
  37.7 1.2 pad_maximum_fusion.1
  38.9 7.6 %collective-permute-start.8 = (bf16[512,1024]{0,1:T(8,128)(2,1)}, bf16[512,1024]{0,1:T(8,128)(2,1)}, u32[]{:S(2)}, u32[]{:S(2)}) collective-permute-start(bf16[512,1024]{0,1:T(8,128)(2,1)} %pad_maximum_fusion.1), channel_id=1, source_target_pairs={{0,8},{2,10},{4,12},{6,14},{8,16},{10,18},{12,20},{14,22},{16,24},... | collective-permute-start | bytes 3145736 | tf_op jit(solution)/shard_map/ppermute | solution.py:10
  46.5 1.4 collective-permute-done.5
  47.9 1.2 pad_maximum_fusion
  49.1 8.6 %collective-permute-start.7 = (bf16[512,1024]{0,1:T(8,128)(2,1)}, bf16[512,1024]{0,1:T(8,128)(2,1)}, u32[]{:S(2)}, u32[]{:S(2)}) collective-permute-start(bf16[512,1024]{0,1:T(8,128)(2,1)} %pad_maximum_fusion), channel_id=1, source_target_pairs={{0,8},{2,10},{4,12},{6,14},{8,16},{10,18},{12,20},{14,22},{16,24},... | collective-permute-start | bytes 3145736 | tf_op jit(solution)/shard_map/ppermute | solution.py:10
  57.7 1.3 collective-permute-start
  59.0 1.3 collective-permute-done
  60.3 5.3 collective-permute-start.1
  65.7 0.7 fusion.51
  66.3 0.6 collective-permute-done.1
  67.0 37.6 %collective-permute-start.2 = (s32[512]{0:T(512)S(1)}, s32[512]{0:T(512)S(1)}, u32[]{:S(2)}, u32[]{:S(2)}) collective-permute-start(s32[512]{0:T(512)S(1)} %pad_add_fusion), channel_id=1, source_target_pairs={{0,8},{2,10},{4,12},{6,14},{8,16},{10,18},{12,20},{14,22},{16,24},... | collective-permute-start | bytes 6152 | tf_op jit(solution)/shard_map/ppermute | solution.py:10
  104.6 0.2 copy.22
  106.1 0.6 slice.76
  107.9 0.7 fusion.50
  111.1 17.5 %conditional.4 = (f32[128,16,64]{0,2,1:T(8,128)S(1)}, f32[16,128]{1,0:T(8,128)S(1)}) conditional(s32[]{:T(128)} %convert_element_type.66, () %tuple.49, (s32[]{:T(128)}, s32[128]{0:T(128)S(1)}, s32[256]{0:T(256)S(1)}, s32[128]{0:T(128)S(1)}, bf16[256,1024]{0,1:T(8,128)(2,1)S(1)}, /*index=5*/bf16[128,16,64]{0,2,1:T(8,128)(2,1)S(1)}, f32[16]{0:T(128)S(1)}, ...), branch_computations={%region_0.0_spmd, %region_1.5_spmd} | conditional | flops 223449856 | bytes 37884532 | solution.py:56
  111.2 0.7 fusion.18
  111.9 1.5 fusion.23
  113.4 2.0 copy.27
  115.4 5.9 fusion.53
  121.3 0.1 broadcast_add_fusion.1
  121.4 1.8 copy.28
  123.3 5.2 convolution_bitcast_fusion.1
  128.5 0.5 conditional.5
  129.0 7.0 conditional.6
  136.0 8.4 %conditional.7 = (f32[128,16,64]{0,2,1:T(8,128)S(1)}) conditional(s32[]{:T(128)} %convert_element_type.63, f32[128,16,64]{0,2,1:T(8,128)S(1)} %get-tuple-element.181, (s32[]{:T(128)}, s32[128]{0:T(128)S(1)}, s32[512]{0:T(512)S(1)}, s32[128]{0:T(128)S(1)}, bf16[512,1024]{0,1:T(8,128)(2,1)}, /*index=5*/bf16[128,16,64]{0,2,1:T(8,128)(2,1)S(1)}, ...), branch_computations={%region_15.16_spmd, %region_16.19_spmd} | conditional | flops 218897152 | bytes 29825692 | solution.py:56
  144.5 3.7 convolution_convert_fusion.1
  148.3 0.5 all-gather.4.cloned.1.call-update
  148.9 0.5 all-gather.6.cloned.1.call-update
  149.5 0.5 all-gather.8.cloned.1.call-update
  150.0 88.4 %reduce-scatter.3.cloned.1.call-done = bf16[64,2048]{1,0:T(8,128)(2,1)} async-done(((bf16[128,2048]{1,0:T(8,128)(2,1)}), bf16[64,2048]{1,0:T(8,128)(2,1)}) %reduce-scatter.3.cloned.1.call-update) | async-done | bytes 262160 | tf_op jit(solution)/shard_map/reduce_scatter | solution.py:100
  238.5 1.1 multiply_reduce_fusion
  239.6 1.1 multiply_convert_fusion
  240.7 2.2 all_gather.12
  242.9 141.8 %all-gather.4.cloned.1.call-done = bf16[2048,3072]{1,0:T(8,128)(2,1)} async-done(((bf16[128,3072]{1,0:T(8,128)(2,1)}), bf16[2048,3072]{1,0:T(8,128)(2,1)}) %all-gather.4.cloned.1.call-update) | async-done | bytes 12582928 | tf_op jit(solution)/shard_map/all_gather | solution.py:113
  384.7 6.4 fusion.56
  391.1 145.5 %all-gather.6.cloned.1.call-done = bf16[2048,3072]{1,0:T(8,128)(2,1)} async-done(((bf16[128,3072]{1,0:T(8,128)(2,1)}), bf16[2048,3072]{1,0:T(8,128)(2,1)}) %all-gather.6.cloned.1.call-update) | async-done | bytes 12582928 | tf_op jit(solution)/shard_map/all_gather | solution.py:118
  536.6 196.1 %all-gather.8.cloned.1.call-done = bf16[3072,2048]{1,0:T(8,128)(2,1)} async-done(((bf16[3072,128]{1,0:T(8,128)(2,1)}), bf16[3072,2048]{1,0:T(8,128)(2,1)}) %all-gather.8.cloned.1.call-update) | async-done | bytes 12582928 | tf_op jit(solution)/shard_map/all_gather | solution.py:124
  732.7 12.7 %convolution_convert_fusion = bf16[128,2048]{1,0:T(8,128)(2,1)} fusion(bf16[3072,2048]{1,0:T(8,128)(2,1)} %all-gather.8.cloned.1.call-done, bf16[128,2048]{1,0:T(8,128)(2,1)S(1)} %all_gather.12, bf16[2048,3072]{1,0:T(8,128)(2,1)} %all-gather.6.cloned.1.call-done, f32[128,3072]{1,0:T(8,128)S(1)} %fusion.56), kind=kOutput, calls=%fused_computation.87 | convolution fusion | flops 3223846912 | bytes 27787264 | tf_op jit(solution)/shard_map/dot_general | solution.py:122
  745.4 6.3 reduce-scatter.5.cloned.1.call-done
  751.7 1.7 add_convert_fusion
  (43 shorter events, 0.6 us)
Async XLA Ops:
  7.4 231.1 %reduce-scatter.3.cloned.1.call-start = ((), (), s32[]{:S(2)}) async-start(), calls=%async_computation.2 | async-start | bytes 786432 | tf_op jit(solution)/shard_map/reduce_scatter | solution.py:100
  8.5 11.6 %collective-permute-start.4 = (bf16[128,1024]{0,1:T(8,128)(2,1)S(1)}, bf16[128,1024]{0,1:T(8,128)(2,1)S(1)}, u32[]{:S(2)}, u32[]{:S(2)}) collective-permute-start(bf16[128,1024]{0,1:T(8,128)(2,1)S(1)} %copy.23), channel_id=1, source_target_pairs={{0,2},{2,4},{4,6},{6,8},{8,10},{10,12},{12,14},{14,16},{16,18},{18... | collective-permute-start | bytes 786440 | tf_op jit(solution)/shard_map/ppermute | solution.py:10
  14.5 11.0 %collective-permute-start.3 = (bf16[128,1024]{0,1:T(8,128)(2,1)S(1)}, bf16[128,1024]{0,1:T(8,128)(2,1)S(1)}, u32[]{:S(2)}, u32[]{:S(2)}) collective-permute-start(bf16[128,1024]{0,1:T(8,128)(2,1)S(1)} %copy.20), channel_id=1, source_target_pairs={{0,2},{2,4},{4,6},{6,8},{8,10},{10,12},{12,14},{14,16},{16,18},{18... | collective-permute-start | bytes 786440 | tf_op jit(solution)/shard_map/ppermute | solution.py:10
  20.1 17.6 %collective-permute-start.6 = (bf16[256,1024]{0,1:T(8,128)(2,1)S(1)}, bf16[256,1024]{0,1:T(8,128)(2,1)S(1)}, u32[]{:S(2)}, u32[]{:S(2)}) collective-permute-start(bf16[256,1024]{0,1:T(8,128)(2,1)S(1)} %pad_maximum_fusion.3), channel_id=1, source_target_pairs={{0,4},{2,6},{4,8},{6,10},{8,12},{10,14},{12,16},{14,18},{16,20},{1... | collective-permute-start | bytes 1572872 | tf_op jit(solution)/shard_map/ppermute | solution.py:10
  25.5 32.2 %copy-start.9 = (s32[128]{0:T(128)S(1)}, s32[128]{0:T(128)}, u32[]{:S(2)}) copy-start(s32[128]{0:T(128)} %param.23) | copy-start | bytes 1540
  25.6 79.1 %copy-start.8 = (bf16[128,1024]{1,0:T(8,128)(2,1)S(1)}, bf16[128,1024]{1,0:T(8,128)(2,1)}, u32[]{:S(2)}) copy-start(bf16[128,1024]{1,0:T(8,128)(2,1)} %param.20) | copy-start | bytes 786436
  25.6 85.5 %copy-start.11 = (f32[16]{0:T(128)S(1)}, f32[16]{0:T(128)}, u32[]{:S(2)}) copy-start(f32[16]{0:T(128)} %param.24) | copy-start | bytes 196
  25.6 22.4 %collective-permute-start.5 = (bf16[256,1024]{0,1:T(8,128)(2,1)S(1)}, bf16[256,1024]{0,1:T(8,128)(2,1)S(1)}, u32[]{:S(2)}, u32[]{:S(2)}) collective-permute-start(bf16[256,1024]{0,1:T(8,128)(2,1)S(1)} %pad_maximum_fusion.2), channel_id=1, source_target_pairs={{0,4},{2,6},{4,8},{6,10},{8,12},{10,14},{12,16},{14,18},{16,20},{1... | collective-permute-start | bytes 1572872 | tf_op jit(solution)/shard_map/ppermute | solution.py:10
  37.7 11.4 %copy-start.5 = (bf16[256,1024]{0,1:T(8,128)(2,1)}, bf16[256,1024]{0,1:T(8,128)(2,1)S(1)}, u32[]{:S(2)}) copy-start(bf16[256,1024]{0,1:T(8,128)(2,1)S(1)} %collective-permute-done.6) | copy-start | bytes 1572868
  38.9 90.1 %collective-permute-start.8 = (bf16[512,1024]{0,1:T(8,128)(2,1)}, bf16[512,1024]{0,1:T(8,128)(2,1)}, u32[]{:S(2)}, u32[]{:S(2)}) collective-permute-start(bf16[512,1024]{0,1:T(8,128)(2,1)} %pad_maximum_fusion.1), channel_id=1, source_target_pairs={{0,8},{2,10},{4,12},{6,14},{8,16},{10,18},{12,20},{14,22},{16,24},... | collective-permute-start | bytes 3145736 | tf_op jit(solution)/shard_map/ppermute | solution.py:10
  47.9 63.1 %copy-start.7 = (bf16[256,1024]{0,1:T(8,128)(2,1)}, bf16[256,1024]{0,1:T(8,128)(2,1)S(1)}, u32[]{:S(2)}) copy-start(bf16[256,1024]{0,1:T(8,128)(2,1)S(1)} %collective-permute-done.5) | copy-start | bytes 1572868
  49.1 79.9 %collective-permute-start.7 = (bf16[512,1024]{0,1:T(8,128)(2,1)}, bf16[512,1024]{0,1:T(8,128)(2,1)}, u32[]{:S(2)}, u32[]{:S(2)}) collective-permute-start(bf16[512,1024]{0,1:T(8,128)(2,1)} %pad_maximum_fusion), channel_id=1, source_target_pairs={{0,8},{2,10},{4,12},{6,14},{8,16},{10,18},{12,20},{14,22},{16,24},... | collective-permute-start | bytes 3145736 | tf_op jit(solution)/shard_map/ppermute | solution.py:10
  57.7 2.6 collective-permute-start
  60.3 6.6 collective-permute-start.1
  67.0 41.0 %collective-permute-start.2 = (s32[512]{0:T(512)S(1)}, s32[512]{0:T(512)S(1)}, u32[]{:S(2)}, u32[]{:S(2)}) collective-permute-start(s32[512]{0:T(512)S(1)} %pad_add_fusion), channel_id=1, source_target_pairs={{0,8},{2,10},{4,12},{6,14},{8,16},{10,18},{12,20},{14,22},{16,24},... | collective-permute-start | bytes 6152 | tf_op jit(solution)/shard_map/ppermute | solution.py:10
  111.9 1.5 copy-start.4
  148.2 90.3 %copy-start = (bf16[64,2048]{1,0:T(8,128)(2,1)S(1)}, bf16[64,2048]{1,0:T(8,128)(2,1)}, u32[]{:S(2)}) copy-start(bf16[64,2048]{1,0:T(8,128)(2,1)} %param.19) | copy-start | bytes 786436
  148.2 91.4 %copy-start.10 = (f32[2048]{0:T(1024)S(1)}, f32[2048]{0:T(1024)}, u32[]{:S(2)}) copy-start(f32[2048]{0:T(1024)} %param.26) | copy-start | bytes 24580
  148.2 236.5 %all-gather.4.cloned.1.call-start = ((), (), s32[]{:S(2)}) async-start(), calls=%async_computation.3 | async-start | bytes 13369344 | tf_op jit(solution)/shard_map/all_gather | solution.py:113
  148.8 387.8 %all-gather.6.cloned.1.call-start = ((), (), s32[]{:S(2)}) async-start(), calls=%async_computation.4 | async-start | bytes 13369344 | tf_op jit(solution)/shard_map/all_gather | solution.py:118
  149.4 583.3 %all-gather.8.cloned.1.call-start = ((), (), s32[]{:S(2)}) async-start(), calls=%async_computation.5 | async-start | bytes 13369344 | tf_op jit(solution)/shard_map/all_gather | solution.py:124
  150.0 601.7 %reduce-scatter.5.cloned.1.call-start = ((), (), s32[]{:S(2)}) async-start(), calls=%async_computation.6 | async-start | bytes 786432 | tf_op jit(solution)/shard_map/reduce_scatter | solution.py:127
  391.1 360.6 %copy-start.1 = (bf16[64,2048]{1,0:T(8,128)(2,1)S(1)}, bf16[64,2048]{1,0:T(8,128)(2,1)}, u32[]{:S(2)}) copy-start(bf16[64,2048]{1,0:T(8,128)(2,1)} %reduce-scatter.3.cloned.1.call-done) | copy-start | bytes 786436
Sparse Core Ops, SparseCore 0:
  148.4 90.0 reduce-scatter.2
  745.5 6.0 reduce-scatter.4
Sparse Core Ops, SparseCore 1:
  151.5 233.2 all-gather.3
  387.4 149.2 all-gather.5
  539.2 193.4 all-gather.7
where the time goes:
time: 771 us; the launch traced here: 761 us
  waiting for transfers between devices  593 us (77%)
  starting transfers between devices  79 us (10%)
  matrix products  28.7 us (4%)
  between operations  20.5 us (3%)
  loops' own time  16 us (2%)
  other arithmetic  14.1 us (2%)
  local copies, waits for them, and re-layouts  8.17 us (1%)
    all_gather x1, waiting for transfers between devices, on_device(): lax.all_gather(down_weight, 'sp', axis=1, tiled=True)  196 us
    all_gather x1, waiting for transfers between devices, on_device(): lax.all_gather(up_weight, 'sp', axis=0, tiled=True)  146 us
    all_gather x1, waiting for transfers between devices, on_device(): lax.all_gather(gate_weight, 'sp', axis=0, tiled=True)  142 us
    reduce_scatter x1, waiting for transfers between devices, on_device(): lax.psum_scatter(jnp.dot(attended, out_weight, preferred_element_type=jnp...  88.4 us
    ppermute x9, starting transfers between devices, from_behind(): return lax.ppermute(shard, axis, pairs)  78.8 us
    another operation x4, loops' own time, block_update(): return lax.cond(reached, compute, lambda: carry)  16 us
  transfers between devices with their start and end apart: 14, of which 10 were waited for; matrix products, arithmetic and copies ran while one was open for 4% of the time, Pallas kernels for 0%

commit v1 on v0

--- a/solution.py
+++ b/solution.py
@@ -115,7 +115,9 @@
     )
     upper = jnp.dot(
         span_rows,
-        lax.all_gather(up_weight, "sp", axis=0, tiled=True),
+        jnp.concatenate(
+            lax.all_to_all(jnp.stack([up_weight] * lax.axis_size("sp")), "sp", 0, 0), axis=0
+        ),
         preferred_element_type=jnp.float32,
     )
     hidden = (jax.nn.silu(gate) * upper).astype(jnp.bfloat16)

time: 771 us -> 859 us (1.11)
  starting transfers between devices: 79 us -> 170 us
    all_gather x1, waiting for transfers between devices: 142 us -> 367 us  [on_device(): lax.all_gather(gate_weight, 'sp', axis=0, tiled=True)]
    all_gather x1 -> x0, waiting for transfers between devices: 146 us -> none  [on_device(): lax.all_gather(up_weight, 'sp', axis=0, tiled=True)]
    all_to_all x0 -> x1, starting transfers between devices: none -> 90.9 us  [on_device(): lax.all_to_all(jnp.stack([up_weight] * lax.axis_size('sp')), 'sp', 0, 0)]
    reduce_scatter x1, waiting for transfers between devices: 88.4 us -> 0.02 us  [on_device(): lax.psum_scatter(jnp.dot(attended, out_weight, preferred_element_type=jnp...]
  transfers between devices with their start and end apart: 14 -> 14, of which waited for: 10 -> 8; matrix products, arithmetic and copies ran while one was open for 4% -> 4% of each run, Pallas kernels for 0% -> 0%
where the time goes in v1:
time: 859 us; the launch traced here: 849 us
  waiting for transfers between devices  587 us (68%)
  starting transfers between devices  170 us (20%)
  matrix products  28.8 us (3%)
  between operations  20.4 us (2%)
  local copies, waits for them, and re-layouts  14.3 us (2%)
  other arithmetic  14.1 us (2%)
  loops' own time  13.1 us (2%)
    all_gather x1, waiting for transfers between devices, on_device(): lax.all_gather(gate_weight, 'sp', axis=0, tiled=True)  367 us
    all_gather x1, waiting for transfers between devices, on_device(): lax.all_gather(down_weight, 'sp', axis=1, tiled=True)  199 us
    all_to_all x1, starting transfers between devices, on_device(): lax.all_to_all(jnp.stack([up_weight] * lax.axis_size('sp')), 'sp', 0, 0)  90.9 us
    ppermute x9, starting transfers between devices, from_behind(): return lax.ppermute(shard, axis, pairs)  78.8 us
  transfers between devices with their start and end apart: 14, of which 8 were waited for; matrix products, arithmetic and copies ran while one was open for 4% of the time, Pallas kernels for 0%

profile of v1, /device:TPU:0, one launch (start us, length us, event | category | flops | bytes accessed | tf_op | source)
XLA Modules:
  0.0 849.5 jit_solution(5705848690438821208)
XLA Ops:
  7.4 1.1 copy.23
  8.5 4.9 collective-permute-start.4
  13.4 1.1 copy.20
  14.5 3.4 collective-permute-start.3
  17.9 2.1 collective-permute-done.4
  20.1 5.3 collective-permute-start.6
  25.6 4.6 collective-permute-start.5
  30.2 7.5 collective-permute-done.6
  37.7 1.2 pad_maximum_fusion.1
  38.9 7.6 collective-permute-start.8
  46.5 1.4 collective-permute-done.5
  47.9 1.2 pad_maximum_fusion
  49.1 8.6 %collective-permute-start.7 = (bf16[512,1024]{0,1:T(8,128)(2,1)}, bf16[512,1024]{0,1:T(8,128)(2,1)}, u32[]{:S(2)}, u32[]{:S(2)}) collective-permute-start(bf16[512,1024]{0,1:T(8,128)(2,1)} %pad_maximum_fusion), channel_id=1, source_target_pairs={{0,8},{2,10},{4,12},{6,14},{8,16},{10,18},{12,20},{14,22},{16,24},... | collective-permute-start | bytes 3145736 | tf_op jit(solution)/shard_map/ppermute | solution.py:10
  57.7 1.3 collective-permute-start
  59.0 1.3 collective-permute-done
  60.3 5.3 collective-permute-start.1
  65.7 0.7 fusion.51
  66.3 0.6 collective-permute-done.1
  67.0 37.7 %collective-permute-start.2 = (s32[512]{0:T(512)S(1)}, s32[512]{0:T(512)S(1)}, u32[]{:S(2)}, u32[]{:S(2)}) collective-permute-start(s32[512]{0:T(512)S(1)} %pad_add_fusion), channel_id=1, source_target_pairs={{0,8},{2,10},{4,12},{6,14},{8,16},{10,18},{12,20},{14,22},{16,24},... | collective-permute-start | bytes 6152 | tf_op jit(solution)/shard_map/ppermute | solution.py:10
  104.6 0.2 copy.22
  106.1 0.6 slice.76
  107.9 0.7 fusion.50
  111.1 17.4 %conditional.4 = (f32[128,16,64]{0,2,1:T(8,128)S(1)}, f32[16,128]{1,0:T(8,128)S(1)}) conditional(s32[]{:T(128)} %convert_element_type.66, () %tuple.49, (s32[]{:T(128)}, s32[128]{0:T(128)S(1)}, s32[256]{0:T(256)S(1)}, s32[128]{0:T(128)S(1)}, bf16[256,1024]{0,1:T(8,128)(2,1)S(1)}, /*index=5*/bf16[128,16,64]{0,2,1:T(8,128)(2,1)S(1)}, f32[16]{0:T(128)S(1)}, ...), branch_computations={%region_0.0_spmd, %region_1.5_spmd} | conditional | flops 223449856 | bytes 37884532 | solution.py:56
  111.1 0.1 compare_and_fusion.1
  111.2 0.7 fusion.18
  111.9 1.5 fusion.23
  113.4 2.0 copy.27
  115.4 5.9 fusion.53
  121.3 0.1 broadcast_add_fusion.1
  121.4 1.8 copy.28
  123.3 5.2 convolution_bitcast_fusion.1
  128.5 0.5 conditional.5
  129.1 7.0 conditional.6
  136.0 5.5 conditional.7
  141.6 3.8 convolution_convert_fusion.1
  145.5 0.5 all-gather.3.cloned.1.call-update
  146.0 6.1 stack.2
  152.1 90.9 %all-to-all-start = ((bf16[16,128,3072]{2,1,0:T(8,128)(2,1)}), bf16[16,128,3072]{2,1,0:T(8,128)(2,1)}, u32[]{:S(2)}, u32[]{:S(2)}) async-start(bf16[16,128,3072]{2,1,0:T(8,128)(2,1)} %stack.2), calls=%async_computation.1 | async-start | bytes 25165824 | tf_op jit(solution)/shard_map/all_to_all | solution.py:119
  243.1 0.5 all-gather.5.cloned.1.call-update
  243.7 1.2 multiply_reduce_fusion
  244.9 1.1 multiply_convert_fusion
  245.9 2.4 all_gather.9
  248.4 367.4 %all-gather.3.cloned.1.call-done = bf16[2048,3072]{1,0:T(8,128)(2,1)} async-done(((bf16[128,3072]{1,0:T(8,128)(2,1)}), bf16[2048,3072]{1,0:T(8,128)(2,1)}) %all-gather.3.cloned.1.call-update) | async-done | bytes 12582928 | tf_op jit(solution)/shard_map/all_gather | solution.py:113
  615.8 6.4 fusion.56
  622.2 198.8 %all-gather.5.cloned.1.call-done = bf16[3072,2048]{1,0:T(8,128)(2,1)} async-done(((bf16[3072,128]{1,0:T(8,128)(2,1)}), bf16[3072,2048]{1,0:T(8,128)(2,1)}) %all-gather.5.cloned.1.call-update) | async-done | bytes 12582928 | tf_op jit(solution)/shard_map/all_gather | solution.py:126
  821.0 12.7 %convolution_convert_fusion = bf16[128,2048]{1,0:T(8,128)(2,1)} fusion(bf16[3072,2048]{1,0:T(8,128)(2,1)} %all-gather.5.cloned.1.call-done, bf16[128,2048]{1,0:T(8,128)(2,1)S(1)} %all_gather.9, bf16[2048,3072]{1,0:T(8,128)(2,1)} %bitcast.24, f32[128,3072]{1,0:T(8,128)S(1)} %fusion.56), kind=kOutput, calls=%fused_computation.87 | convolution fusion | flops 3223846912 | bytes 27787264 | tf_op jit(solution)/shard_map/dot_general | solution.py:124
  833.8 6.3 reduce-scatter.5.cloned.1.call-done
  840.0 1.7 add_convert_fusion
  (45 shorter events, 0.5 us)
Async XLA Ops:
  7.4 236.3 %reduce-scatter.3.cloned.1.call-start = ((), (), s32[]{:S(2)}) async-start(), calls=%async_computation.3 | async-start | bytes 786432 | tf_op jit(solution)/shard_map/reduce_scatter | solution.py:100
  8.5 11.6 %collective-permute-start.4 = (bf16[128,1024]{0,1:T(8,128)(2,1)S(1)}, bf16[128,1024]{0,1:T(8,128)(2,1)S(1)}, u32[]{:S(2)}, u32[]{:S(2)}) collective-permute-start(bf16[128,1024]{0,1:T(8,128)(2,1)S(1)} %copy.23), channel_id=1, source_target_pairs={{0,2},{2,4},{4,6},{6,8},{8,10},{10,12},{12,14},{14,16},{16,18},{18... | collective-permute-start | bytes 786440 | tf_op jit(solution)/shard_map/ppermute | solution.py:10
  14.5 11.0 %collective-permute-start.3 = (bf16[128,1024]{0,1:T(8,128)(2,1)S(1)}, bf16[128,1024]{0,1:T(8,128)(2,1)S(1)}, u32[]{:S(2)}, u32[]{:S(2)}) collective-permute-start(bf16[128,1024]{0,1:T(8,128)(2,1)S(1)} %copy.20), channel_id=1, source_target_pairs={{0,2},{2,4},{4,6},{6,8},{8,10},{10,12},{12,14},{14,16},{16,18},{18... | collective-permute-start | bytes 786440 | tf_op jit(solution)/shard_map/ppermute | solution.py:10
  20.1 17.6 %collective-permute-start.6 = (bf16[256,1024]{0,1:T(8,128)(2,1)S(1)}, bf16[256,1024]{0,1:T(8,128)(2,1)S(1)}, u32[]{:S(2)}, u32[]{:S(2)}) collective-permute-start(bf16[256,1024]{0,1:T(8,128)(2,1)S(1)} %pad_maximum_fusion.3), channel_id=1, source_target_pairs={{0,4},{2,6},{4,8},{6,10},{8,12},{10,14},{12,16},{14,18},{16,20},{1... | collective-permute-start | bytes 1572872 | tf_op jit(solution)/shard_map/ppermute | solution.py:10
  25.5 32.2 %copy-start.10 = (s32[128]{0:T(128)S(1)}, s32[128]{0:T(128)}, u32[]{:S(2)}) copy-start(s32[128]{0:T(128)} %param.23) | copy-start | bytes 1540
  25.6 79.1 %copy-start.9 = (bf16[128,1024]{1,0:T(8,128)(2,1)S(1)}, bf16[128,1024]{1,0:T(8,128)(2,1)}, u32[]{:S(2)}) copy-start(bf16[128,1024]{1,0:T(8,128)(2,1)} %param.20) | copy-start | bytes 786436
  25.6 85.5 %copy-start.12 = (f32[16]{0:T(128)S(1)}, f32[16]{0:T(128)}, u32[]{:S(2)}) copy-start(f32[16]{0:T(128)} %param.24) | copy-start | bytes 196
  25.6 22.4 %collective-permute-start.5 = (bf16[256,1024]{0,1:T(8,128)(2,1)S(1)}, bf16[256,1024]{0,1:T(8,128)(2,1)S(1)}, u32[]{:S(2)}, u32[]{:S(2)}) collective-permute-start(bf16[256,1024]{0,1:T(8,128)(2,1)S(1)} %pad_maximum_fusion.2), channel_id=1, source_target_pairs={{0,4},{2,6},{4,8},{6,10},{8,12},{10,14},{12,16},{14,18},{16,20},{1... | collective-permute-start | bytes 1572872 | tf_op jit(solution)/shard_map/ppermute | solution.py:10
  37.7 21.3 %copy-start.6 = (bf16[256,1024]{0,1:T(8,128)(2,1)}, bf16[256,1024]{0,1:T(8,128)(2,1)S(1)}, u32[]{:S(2)}) copy-start(bf16[256,1024]{0,1:T(8,128)(2,1)S(1)} %collective-permute-done.6) | copy-start | bytes 1572868
  38.9 90.2 %collective-permute-start.8 = (bf16[512,1024]{0,1:T(8,128)(2,1)}, bf16[512,1024]{0,1:T(8,128)(2,1)}, u32[]{:S(2)}, u32[]{:S(2)}) collective-permute-start(bf16[512,1024]{0,1:T(8,128)(2,1)} %pad_maximum_fusion.1), channel_id=1, source_target_pairs={{0,8},{2,10},{4,12},{6,14},{8,16},{10,18},{12,20},{14,22},{16,24},... | collective-permute-start | bytes 3145736 | tf_op jit(solution)/shard_map/ppermute | solution.py:10
  47.9 63.1 %copy-start.8 = (bf16[256,1024]{0,1:T(8,128)(2,1)}, bf16[256,1024]{0,1:T(8,128)(2,1)S(1)}, u32[]{:S(2)}) copy-start(bf16[256,1024]{0,1:T(8,128)(2,1)S(1)} %collective-permute-done.5) | copy-start | bytes 1572868
  49.1 80.0 %collective-permute-start.7 = (bf16[512,1024]{0,1:T(8,128)(2,1)}, bf16[512,1024]{0,1:T(8,128)(2,1)}, u32[]{:S(2)}, u32[]{:S(2)}) collective-permute-start(bf16[512,1024]{0,1:T(8,128)(2,1)} %pad_maximum_fusion), channel_id=1, source_target_pairs={{0,8},{2,10},{4,12},{6,14},{8,16},{10,18},{12,20},{14,22},{16,24},... | collective-permute-start | bytes 3145736 | tf_op jit(solution)/shard_map/ppermute | solution.py:10
  57.7 2.6 collective-permute-start
  60.3 6.6 collective-permute-start.1
  67.0 41.0 %collective-permute-start.2 = (s32[512]{0:T(512)S(1)}, s32[512]{0:T(512)S(1)}, u32[]{:S(2)}, u32[]{:S(2)}) collective-permute-start(s32[512]{0:T(512)S(1)} %pad_add_fusion), channel_id=1, source_target_pairs={{0,8},{2,10},{4,12},{6,14},{8,16},{10,18},{12,20},{14,22},{16,24},... | collective-permute-start | bytes 6152 | tf_op jit(solution)/shard_map/ppermute | solution.py:10
  111.9 1.5 copy-start.4
  141.6 4.4 copy-start.5
  145.4 470.4 %all-gather.3.cloned.1.call-start = ((), (), s32[]{:S(2)}) async-start(), calls=%async_computation.4 | async-start | bytes 13369344 | tf_op jit(solution)/shard_map/all_gather | solution.py:113
  152.1 91.6 %copy-start = (bf16[64,2048]{1,0:T(8,128)(2,1)S(1)}, bf16[64,2048]{1,0:T(8,128)(2,1)}, u32[]{:S(2)}) copy-start(bf16[64,2048]{1,0:T(8,128)(2,1)} %param.19) | copy-start | bytes 786436
  152.1 92.7 %copy-start.11 = (f32[2048]{0:T(1024)S(1)}, f32[2048]{0:T(1024)}, u32[]{:S(2)}) copy-start(f32[2048]{0:T(1024)} %param.26) | copy-start | bytes 24580
  152.1 470.1 %all-to-all-start = ((bf16[16,128,3072]{2,1,0:T(8,128)(2,1)}), bf16[16,128,3072]{2,1,0:T(8,128)(2,1)}, u32[]{:S(2)}, u32[]{:S(2)}) async-start(bf16[16,128,3072]{2,1,0:T(8,128)(2,1)} %stack.2), calls=%async_computation.1 | async-start | bytes 25165824 | tf_op jit(solution)/shard_map/all_to_all | solution.py:119
  243.0 578.0 %all-gather.5.cloned.1.call-start = ((), (), s32[]{:S(2)}) async-start(), calls=%async_computation.5 | async-start | bytes 13369344 | tf_op jit(solution)/shard_map/all_gather | solution.py:126
  243.6 596.4 %reduce-scatter.5.cloned.1.call-start = ((), (), s32[]{:S(2)}) async-start(), calls=%async_computation.6 | async-start | bytes 786432 | tf_op jit(solution)/shard_map/reduce_scatter | solution.py:129
  821.0 19.0 %copy-start.1 = (bf16[64,2048]{1,0:T(8,128)(2,1)S(1)}, bf16[64,2048]{1,0:T(8,128)(2,1)}, u32[]{:S(2)}) copy-start(bf16[64,2048]{1,0:T(8,128)(2,1)} %reduce-scatter.3.cloned.1.call-done) | copy-start | bytes 786436
Sparse Core Ops, SparseCore 0:
  145.5 93.0 reduce-scatter.2
  833.9 6.0 reduce-scatter.4
Sparse Core Ops, SparseCore 1:
  148.7 467.1 all-gather.2
  618.4 202.6 all-gather.4
